TPU v7x, 32 devices: a whole 2x2x4 slice. The times are simulated.
32 devices in a mesh: rep: 2 (over x), fs: 8 (over z, y), tp: 2 (over core).
Axes of the slice: x: 2, y: 2, z: 4, core: 2. Of those that a mesh axis runs over, the one named last changes fastest.
Arguments:
- tokens: bfloat16 [5120, 2048], P(('rep', 'fs')), may hold values from -6 to 6
- mixer_out: bfloat16 [5120, 2048], P(('rep', 'fs')), may hold values from -6 to 6
- gate_first: bfloat16 [2048, 2816], P('fs', 'tp'), may hold values from -0.125 to 0.125
- up_first: bfloat16 [2048, 2816], P('fs', 'tp'), may hold values from -0.125 to 0.125
- down_first: bfloat16 [2816, 2048], P('tp', 'fs'), may hold values from -0.3125 to 0.3125
- gate_second: bfloat16 [2048, 2816], P('fs', 'tp'), may hold values from -0.125 to 0.125
- up_second: bfloat16 [2048, 2816], P('fs', 'tp'), may hold values from -0.125 to 0.125
- down_second: bfloat16 [2816, 2048], P('tp', 'fs'), may hold values from -0.3125 to 0.3125
- gain_first: float32 [2048], replicated, may hold values from 0.1 to 1.9
- bias_first: float32 [2048], replicated, may hold values from -1.5 to 1.5
- gain_middle: float32 [2048], replicated, may hold values from 0.1 to 1.9
- bias_middle: float32 [2048], replicated, may hold values from -1.5 to 1.5
- gain_last: float32 [2048], replicated, may hold values from 0.1 to 1.9
- bias_last: float32 [2048], replicated, may hold values from -1.5 to 1.5
Outputs:
- layer_out: bfloat16 [5120, 2048], P(('rep', 'fs'))
All inputs are finite; a program needn't handle non-finite values.
Results may differ from a plain program's by a relative error of at most 0.014.
Values may be sent and summed in bfloat16 or wider, within the bound.
A program may use at most 64 MiB of HBM per device.

v0:
```python
import math
import jax
import jax.numpy as jnp
from jax import lax
from jax.sharding import PartitionSpec as P

residual_scale = math.sqrt(2.0)
norm_eps = 1e-05


def normalize(summed, scaling, offset):
    center = summed - jnp.mean(summed, axis=-1, keepdims=True)
    spread = jnp.mean(center * center, axis=-1, keepdims=True)
    return center * lax.rsqrt(spread + norm_eps) * scaling + offset


def add_columns(inputs, portion):
    return jnp.dot(inputs, portion, preferred_element_type=jnp.float32)


def project_in(inputs, gate_weight, up_weight):
    return (
        add_columns(inputs, lax.all_gather(gate_weight, "fs", axis=0, tiled=True)),
        add_columns(inputs, lax.all_gather(up_weight, "fs", axis=0, tiled=True)),
    )


def project_out(hidden, down_weight):
    return jnp.dot(
        hidden,
        lax.all_gather(down_weight, "fs", axis=1, tiled=True),
        preferred_element_type=jnp.float32,
    )


def half_step(inputs, gate_weight, up_weight, down_weight):
    gate, value = project_in(inputs, gate_weight, up_weight)
    hidden = (jax.nn.silu(gate) * value).astype(jnp.bfloat16)
    partials = project_out(hidden, down_weight)
    summed = lax.psum(partials.astype(jnp.bfloat16), "tp")
    return summed


def per_device(
    tokens,
    mixer_out,
    gate_first,
    up_first,
    down_first,
    gate_second,
    up_second,
    down_second,
    gain_first,
    bias_first,
    gain_middle,
    bias_middle,
    gain_last,
    bias_last,
):
    first_branch = half_step(tokens, gate_first, up_first, down_first)
    first_norm = normalize(
        residual_scale * tokens.astype(jnp.float32) + 0.5 * first_branch.astype(jnp.float32),
        gain_first,
        bias_first,
    ).astype(jnp.bfloat16)
    middle_norm = normalize(
        residual_scale * first_norm.astype(jnp.float32) + mixer_out.astype(jnp.float32),
        gain_middle,
        bias_middle,
    ).astype(jnp.bfloat16)
    second_branch = half_step(middle_norm, gate_second, up_second, down_second)
    finished = normalize(
        residual_scale * middle_norm.astype(jnp.float32) + 0.5 * second_branch.astype(jnp.float32),
        gain_last,
        bias_last,
    ).astype(jnp.bfloat16)
    return finished


def solution(mesh):
    return jax.shard_map(
        per_device,
        mesh=mesh,
        in_specs=(
            P(("rep", "fs"), None),
            P(("rep", "fs"), None),
            P("fs", "tp"),
            P("fs", "tp"),
            P("tp", "fs"),
            P("fs", "tp"),
            P("fs", "tp"),
            P("tp", "fs"),
            P(),
            P(),
            P(),
            P(),
            P(),
            P(),
        ),
        out_specs=P(("rep", "fs"), None),
        check_vma=False,
    )
```

profile of v0, /device:TPU:0, one launch (start us, length us, event | category | flops | bytes accessed | tf_op | source)
XLA Modules:
  0.0 639.6 jit_solution(13720102844049315975)
XLA Ops:
  6.5 0.7 all-gather.7.cloned.1.call-update
  7.3 0.7 all-gather.11.cloned.1.call-update
  8.0 0.0 all-gather.9.cloned.1.call-start
  8.1 0.7 all-gather.9.cloned.1.call-update
  8.8 0.0 all-reduce.3.cloned.1.call-start
  8.8 95.8 %all-gather.7.cloned.1.call-done = bf16[2048,1408]{1,0:T(8,128)(2,1)} async-done(((bf16[256,1408]{1,0:T(8,128)(2,1)}), bf16[2048,1408]{1,0:T(8,128)(2,1)}) %all-gather.7.cloned.1.call-update) | async-done | bytes 5767184 | tf_op jit(solution)/shard_map/all_gather | solution.py:23
  104.6 5.2 fusion.7
  109.8 88.2 %all-gather.11.cloned.1.call-done = bf16[1408,2048]{1,0:T(8,128)(2,1)} async-done(((bf16[1408,256]{1,0:T(8,128)(2,1)}), bf16[1408,2048]{1,0:T(8,128)(2,1)}) %all-gather.11.cloned.1.call-update) | async-done | bytes 5767184 | tf_op jit(solution)/shard_map/all_gather | solution.py:31
  198.0 92.7 %all-gather.9.cloned.1.call-done = bf16[2048,1408]{1,0:T(8,128)(2,1)} async-done(((bf16[256,1408]{1,0:T(8,128)(2,1)}), bf16[2048,1408]{1,0:T(8,128)(2,1)}) %all-gather.9.cloned.1.call-update) | async-done | bytes 5767184 | tf_op jit(solution)/shard_map/all_gather | solution.py:24
  290.7 9.7 %convolution_convert_fusion.1 = bf16[320,2048]{1,0:T(8,128)(2,1)} fusion(bf16[1408,2048]{1,0:T(8,128)(2,1)} %all-gather.11.cloned.1.call-done, bf16[320,2048]{1,0:T(8,128)(2,1)S(1)} %copy-done.2, bf16[2048,1408]{1,0:T(8,128)(2,1)} %all-gather.9.cloned.1.call-done, f32[320,1408]{1,0:T(8,128)S(1)} %fusion.7), kind=kOutput, calls=%fused_computation.3 | convolution fusion | flops 3694346240 | bytes 15958016 | tf_op jit(solution)/shard_map/dot_general | solution.py:29
  300.4 0.0 all-gather.13.cloned.1.call-start
  300.4 0.5 all-gather.13.cloned.1.call-update
  301.0 0.0 all-gather.15.cloned.1.call-start
  301.0 0.5 all-gather.15.cloned.1.call-update
  301.5 0.0 all-gather.17.cloned.1.call-start
  301.6 0.7 all-gather.17.cloned.1.call-update
  302.3 0.2 all-reduce.5.cloned.1.call-start
  302.5 16.1 %all-reduce.3.cloned.1.call-done = bf16[320,2048]{1,0:T(8,128)(2,1)} async-done(((bf16[320,2048]{1,0:T(8,128)(2,1)}), bf16[320,2048]{1,0:T(8,128)(2,1)}) %all-reduce.3.cloned.1.call-update) | async-done | bytes 1310736 | tf_op jit(solution)/shard_map/psum | solution.py:40
  318.6 2.0 fusion.3
  320.6 0.8 multiply_reduce_fusion.2
  321.5 1.3 fusion.2
  322.8 0.7 multiply_reduce_fusion.1
  323.5 0.8 add_convert_fusion.1
  324.3 89.9 %all-gather.13.cloned.1.call-done = bf16[2048,1408]{1,0:T(8,128)(2,1)} async-done(((bf16[256,1408]{1,0:T(8,128)(2,1)}), bf16[2048,1408]{1,0:T(8,128)(2,1)}) %all-gather.13.cloned.1.call-update) | async-done | bytes 5767184 | tf_op jit(solution)/shard_map/all_gather | solution.py:23
  414.2 4.8 fusion.8
  419.0 87.7 %all-gather.15.cloned.1.call-done = bf16[2048,1408]{1,0:T(8,128)(2,1)} async-done(((bf16[256,1408]{1,0:T(8,128)(2,1)}), bf16[2048,1408]{1,0:T(8,128)(2,1)}) %all-gather.15.cloned.1.call-update) | async-done | bytes 5767184 | tf_op jit(solution)/shard_map/all_gather | solution.py:24
  506.7 93.4 %all-gather.17.cloned.1.call-done = bf16[1408,2048]{1,0:T(8,128)(2,1)} async-done(((bf16[1408,256]{1,0:T(8,128)(2,1)}), bf16[1408,2048]{1,0:T(8,128)(2,1)}) %all-gather.17.cloned.1.call-update) | async-done | bytes 5767184 | tf_op jit(solution)/shard_map/all_gather | solution.py:31
  600.1 9.7 %convolution_convert_fusion = bf16[320,2048]{1,0:T(8,128)(2,1)} fusion(bf16[1408,2048]{1,0:T(8,128)(2,1)} %all-gather.17.cloned.1.call-done, bf16[320,2048]{1,0:T(8,128)(2,1)S(1)} %add_convert_fusion.1, bf16[2048,1408]{1,0:T(8,128)(2,1)} %all-gather.15.cloned.1.call-done, f32[320,1408]{1,0:T(8,128)S(1)} %fusion.8), kind=kOutput, calls=%fused_computation.2 | convolution fusion | flops 3694346240 | bytes 15958016 | tf_op jit(solution)/shard_map/dot_general | solution.py:29
  609.8 18.2 %all-reduce.5.cloned.1.call-done = bf16[320,2048]{1,0:T(8,128)(2,1)} async-done(((bf16[320,2048]{1,0:T(8,128)(2,1)}), bf16[320,2048]{1,0:T(8,128)(2,1)}) %all-reduce.5.cloned.1.call-update) | async-done | bytes 1310736 | tf_op jit(solution)/shard_map/psum | solution.py:40
  628.0 2.0 fusion.4
  630.0 0.8 multiply_reduce_fusion
  630.9 1.9 add_convert_fusion
  (30 shorter events, 0.2 us)
Async XLA Ops:
  6.5 98.0 %all-gather.7.cloned.1.call-start = ((), (), s32[]{:S(2)}) async-start(), calls=%async_computation | async-start | bytes 6488064 | tf_op jit(solution)/shard_map/all_gather | solution.py:23
  7.3 190.7 %all-gather.11.cloned.1.call-start = ((), (), s32[]{:S(2)}) async-start(), calls=%async_computation.2 | async-start | bytes 6488064 | tf_op jit(solution)/shard_map/all_gather | solution.py:31
  8.0 282.7 %all-gather.9.cloned.1.call-start = ((), (), s32[]{:S(2)}) async-start(), calls=%async_computation.1 | async-start | bytes 6488064 | tf_op jit(solution)/shard_map/all_gather | solution.py:24
  8.7 281.9 %copy-start.2 = (bf16[320,2048]{1,0:T(8,128)(2,1)S(1)}, bf16[320,2048]{1,0:T(8,128)(2,1)}, u32[]{:S(2)}) copy-start(bf16[320,2048]{1,0:T(8,128)(2,1)} %param.14) | copy-start | bytes 3932164
  8.8 309.8 %all-reduce.3.cloned.1.call-start = ((), (), s32[]{:S(2)}) async-start(), calls=%async_computation.3 | async-start | bytes 2621440 | tf_op jit(solution)/shard_map/psum | solution.py:40
  300.4 113.8 %all-gather.13.cloned.1.call-start = ((), (), s32[]{:S(2)}) async-start(), calls=%async_computation.4 | async-start | bytes 6488064 | tf_op jit(solution)/shard_map/all_gather | solution.py:23
  301.0 205.8 %all-gather.15.cloned.1.call-start = ((), (), s32[]{:S(2)}) async-start(), calls=%async_computation.5 | async-start | bytes 6488064 | tf_op jit(solution)/shard_map/all_gather | solution.py:24
  301.5 298.6 %all-gather.17.cloned.1.call-start = ((), (), s32[]{:S(2)}) async-start(), calls=%async_computation.6 | async-start | bytes 6488064 | tf_op jit(solution)/shard_map/all_gather | solution.py:31
  301.6 19.9 %copy-start.4 = (f32[2048]{0:T(1024)S(1)}, f32[2048]{0:T(1024)}, u32[]{:S(2)}) copy-start(f32[2048]{0:T(1024)} %param.23) | copy-start | bytes 24580
  301.6 19.9 %copy-start.5 = (f32[2048]{0:T(1024)S(1)}, f32[2048]{0:T(1024)}, u32[]{:S(2)}) copy-start(f32[2048]{0:T(1024)} %param.22) | copy-start | bytes 24580
  302.3 19.2 %copy-start.1 = (bf16[320,2048]{1,0:T(8,128)(2,1)S(1)}, bf16[320,2048]{1,0:T(8,128)(2,1)}, u32[]{:S(2)}) copy-start(bf16[320,2048]{1,0:T(8,128)(2,1)} %param.15) | copy-start | bytes 3932164
  302.3 325.7 %all-reduce.5.cloned.1.call-start = ((), (), s32[]{:S(2)}) async-start(), calls=%async_computation.7 | async-start | bytes 2621440 | tf_op jit(solution)/shard_map/psum | solution.py:40
  318.6 2.0 copy-start.3
  322.8 0.7 copy-start.6
  322.8 0.7 copy-start.7
  609.8 21.0 %copy-start.8 = (f32[2048]{0:T(1024)S(1)}, f32[2048]{0:T(1024)}, u32[]{:S(2)}) copy-start(f32[2048]{0:T(1024)} %param.27) | copy-start | bytes 24580
  609.8 21.0 %copy-start.9 = (f32[2048]{0:T(1024)S(1)}, f32[2048]{0:T(1024)}, u32[]{:S(2)}) copy-start(f32[2048]{0:T(1024)} %param.26) | copy-start | bytes 24580
  628.0 2.0 copy-start
Sparse Core Ops, SparseCore 0:
  9.5 95.0 all-gather.6
  106.6 91.3 all-gather.10
  200.2 90.4 all-gather.8
  300.5 18.0 all-reduce.2
  320.6 93.4 all-gather.12
  416.2 90.4 all-gather.14
  508.8 91.2 all-gather.16
  609.9 18.0 all-reduce.4
where the time goes:
time: 640 us
  waiting for transfers between devices  586 us (92%)
  matrix products  29.4 us (5%)
  between operations  13.6 us (2%)
  other arithmetic  10.4 us (2%)
    all_gather x2, waiting for transfers between devices, project_in(): lax.all_gather(gate_weight, 'fs', axis=0, tiled=True)  186 us
    all_gather x2, waiting for transfers between devices, project_out(): lax.all_gather(down_weight, 'fs', axis=1, tiled=True)  182 us
    all_gather x2, waiting for transfers between devices, project_in(): lax.all_gather(up_weight, 'fs', axis=0, tiled=True)  180 us
    psum x2, waiting for transfers between devices, half_step(): summed = lax.psum(partials.astype(jnp.bfloat16), 'tp')  34.3 us
    dot_general x2, matrix products, project_out(): jnp.dot(hidden, lax.all_gather(down_weight, 'fs', axis=1, tiled=True), pr...  19.3 us
  transfers between devices with their start and end apart: 8, of which 8 were waited for; matrix products, arithmetic and copies ran while one was open for 2% of the time, Pallas kernels for 0%

commit v1 on v0

--- a/solution.py
+++ b/solution.py
@@ -19,8 +19,23 @@
 
 
 def project_in(inputs, gate_weight, up_weight):
+
+    def derive_record(z, ax_name):
+        n_slots = lax.axis_size(ax_name)
+        tray = [(jj, (jj + 1) % n_slots) for jj in range(n_slots)]
+        near, newest = ([z], [z])
+        trail = [(jj, (jj - 1) % n_slots) for jj in range(n_slots)]
+        for _ in range(n_slots // 2):
+            near.append(lax.ppermute(near[-1], ax_name, tray))
+        c = 0
+        while c < (n_slots - 1) // 2:
+            newest.append(lax.ppermute(newest[-1], ax_name, trail))
+            c += 1
+        val2 = jnp.concatenate([*near[::-1], *newest[1:]], axis=0)
+        return jnp.roll(val2, (lax.axis_index(ax_name) - n_slots // 2) * z.shape[0], axis=0)
+
     return (
-        add_columns(inputs, lax.all_gather(gate_weight, "fs", axis=0, tiled=True)),
+        add_columns(inputs, derive_record(gate_weight, ax_name="fs")),
         add_columns(inputs, lax.all_gather(up_weight, "fs", axis=0, tiled=True)),
     )
 

time: 640 us -> 592 us (0.925)
  waiting for transfers between devices: 586 us -> 455 us
  starting transfers between devices: 0.45 us -> 64.2 us
  local copies, waits for them, and re-layouts: 0.05 us -> 17.2 us
    ppermute x0 -> x14, waiting for transfers between devices: none -> 237 us  [the longest x8 237 us: derive_record(): near.append(lax.ppermute(near[-1], ax_name, tray))]
    all_gather x2 -> x0, waiting for transfers between devices: 186 us -> none  [project_in(): lax.all_gather(gate_weight, 'fs', axis=0, tiled=True)]
    all_gather x2, waiting for transfers between devices: 180 us -> 19.3 us  [project_in(): lax.all_gather(up_weight, 'fs', axis=0, tiled=True)]
    ppermute x0 -> x14, starting transfers between devices: none -> 64 us  [the longest x6 50.7 us: derive_record(): newest.append(lax.ppermute(newest[-1], ax_name, trail))]
    psum x2, waiting for transfers between devices: 34.3 us -> 18.2 us  [half_step(): summed = lax.psum(partials.astype(jnp.bfloat16), 'tp')]
    unnamed x20 -> x38, local copies, waits for them, and re-layouts: 0.05 us -> 15.3 us
  transfers between devices with their start and end apart: 8 -> 20, of which waited for: 8 -> 13; matrix products, arithmetic and copies ran while one was open for 2% -> 5% of each run, Pallas kernels for 0% -> 0%
where the time goes in v1:
time: 592 us
  waiting for transfers between devices  455 us (77%)
  starting transfers between devices  64.2 us (11%)
  matrix products  31.2 us (5%)
  local copies, waits for them, and re-layouts  17.2 us (3%)
  between operations  13.6 us (2%)
  other arithmetic  10.4 us (2%)
    ppermute x8, waiting for transfers between devices, derive_record(): near.append(lax.ppermute(near[-1], ax_name, tray))  237 us
    all_gather x2, waiting for transfers between devices, project_out(): lax.all_gather(down_weight, 'fs', axis=1, tiled=True)  179 us
    ppermute x6, starting transfers between devices, derive_record(): newest.append(lax.ppermute(newest[-1], ax_name, trail))  50.7 us
    dot_general x2, matrix products, project_out(): jnp.dot(hidden, lax.all_gather(down_weight, 'fs', axis=1, tiled=True), pr...  21.5 us
    all_gather x2, waiting for transfers between devices, project_in(): lax.all_gather(up_weight, 'fs', axis=0, tiled=True)  19.3 us
    psum x2, waiting for transfers between devices, half_step(): summed = lax.psum(partials.astype(jnp.bfloat16), 'tp')  18.2 us
    unnamed x38, local copies, waits for them, and re-layouts  15.3 us
    ppermute x8, starting transfers between devices, derive_record(): near.append(lax.ppermute(near[-1], ax_name, tray))  13.4 us
  transfers between devices with their start and end apart: 20, of which 13 were waited for; matrix products, arithmetic and copies ran while one was open for 5% of the time, Pallas kernels for 0%

profile of v1, /device:TPU:0, one launch (start us, length us, event | category | flops | bytes accessed | tf_op | source)
XLA Modules:
  0.0 592.0 jit_solution(7408308319202359925)
XLA Ops:
  8.1 3.0 collective-permute-start
  11.1 24.5 %collective-permute-done = bf16[256,1408]{1,0:T(8,128)(2,1)S(1)} collective-permute-done((bf16[256,1408]{1,0:T(8,128)(2,1)}, bf16[256,1408]{1,0:T(8,128)(2,1)S(1)}, u32[]{:S(2)}, u32[]{:S(2)}) %collective-permute-start) | collective-permute-done | bytes 720928 | tf_op jit(solution)/shard_map/ppermute | solution.py:29
  36.1 4.3 collective-permute-start.4
  40.3 28.9 %collective-permute-done.1 = bf16[256,1408]{1,0:T(8,128)(2,1)S(1)} collective-permute-done((bf16[256,1408]{1,0:T(8,128)(2,1)S(1)}, bf16[256,1408]{1,0:T(8,128)(2,1)S(1)}, u32[]{:S(2)}, u32[]{:S(2)}) %collective-permute-start.1) | collective-permute-done | bytes 720928 | tf_op jit(solution)/shard_map/ppermute | solution.py:29
  69.2 13.8 %collective-permute-start.5 = (bf16[256,1408]{1,0:T(8,128)(2,1)S(1)}, bf16[256,1408]{1,0:T(8,128)(2,1)S(1)}, u32[]{:S(2)}, u32[]{:S(2)}) collective-permute-start(bf16[256,1408]{1,0:T(8,128)(2,1)S(1)} %collective-permute-done.4), channel_id=1, source_target_pairs={{0,14},{2,0},{4,2},{6,4},{8,6},{10,8},{12,10},{14,12},{1,15},{3,1}... | collective-permute-start | bytes 2162696 | tf_op jit(solution)/shard_map/ppermute | solution.py:32
  83.0 32.0 %collective-permute-done.2 = bf16[256,1408]{1,0:T(8,128)(2,1)} collective-permute-done((bf16[256,1408]{1,0:T(8,128)(2,1)S(1)}, bf16[256,1408]{1,0:T(8,128)(2,1)}, u32[]{:S(2)}, u32[]{:S(2)}) %collective-permute-start.2) | collective-permute-done | bytes 720928 | tf_op jit(solution)/shard_map/ppermute | solution.py:29
  115.0 2.6 collective-permute-start.3
  117.6 24.3 %collective-permute-start.6 = (bf16[256,1408]{1,0:T(8,128)(2,1)S(1)}, bf16[256,1408]{1,0:T(8,128)(2,1)S(1)}, u32[]{:S(2)}, u32[]{:S(2)}) collective-permute-start(bf16[256,1408]{1,0:T(8,128)(2,1)S(1)} %collective-permute-done.5), channel_id=1, source_target_pairs={{0,14},{2,0},{4,2},{6,4},{8,6},{10,8},{12,10},{14,12},{1,15},{3,1}... | collective-permute-start | bytes 2162696 | tf_op jit(solution)/shard_map/ppermute | solution.py:32
  141.9 19.6 %collective-permute-done.3 = bf16[256,1408]{1,0:T(8,128)(2,1)} collective-permute-done((bf16[256,1408]{1,0:T(8,128)(2,1)}, bf16[256,1408]{1,0:T(8,128)(2,1)}, u32[]{:S(2)}, u32[]{:S(2)}) %collective-permute-start.3) | collective-permute-done | bytes 720928 | tf_op jit(solution)/shard_map/ppermute | solution.py:29
  161.5 2.1 constant_dynamic-update-slice_fusion.7
  163.6 2.0 constant_dynamic-update-slice_fusion.6
  171.2 7.7 %all-gather.5.cloned.1.call-done = bf16[2048,1408]{1,0:T(8,128)(2,1)} async-done(((bf16[256,1408]{1,0:T(8,128)(2,1)}), bf16[2048,1408]{1,0:T(8,128)(2,1)}) %all-gather.5.cloned.1.call-update) | async-done | bytes 5767184 | tf_op jit(solution)/shard_map/all_gather | solution.py:39
  178.9 4.8 fusion.32
  183.7 90.2 %all-gather.7.cloned.1.call-done = bf16[1408,2048]{1,0:T(8,128)(2,1)} async-done(((bf16[1408,256]{1,0:T(8,128)(2,1)}), bf16[1408,2048]{1,0:T(8,128)(2,1)}) %all-gather.7.cloned.1.call-update) | async-done | bytes 5767184 | tf_op jit(solution)/shard_map/all_gather | solution.py:46
  273.9 10.8 %convolution_convert_fusion.1 = bf16[320,2048]{1,0:T(8,128)(2,1)} fusion(bf16[1408,2048]{1,0:T(8,128)(2,1)} %all-gather.7.cloned.1.call-done, f32[320,1408]{1,0:T(8,128)S(1)} %fusion.32, bf16[320,2048]{1,0:T(8,128)(2,1)S(1)} %copy-done.2, s32[]{:T(128)S(6)} %select_n.13, bf16[2048,1408]{1,0:T(8,128)(2,1)} %constant_dynamic-update-slice_fusion), kind=kOutput, calls=%fused_computation.10 | convolution fusion | flops 3705880576 | bytes 15958020 | tf_op jit(solution)/shard_map/dot_general | solution.py:44
  286.0 1.5 collective-permute-start.7
  287.4 18.4 %collective-permute-done.7 = bf16[256,1408]{1,0:T(8,128)(2,1)S(1)} collective-permute-done((bf16[256,1408]{1,0:T(8,128)(2,1)S(1)}, bf16[256,1408]{1,0:T(8,128)(2,1)S(1)}, u32[]{:S(2)}, u32[]{:S(2)}) %collective-permute-start.7) | collective-permute-done | bytes 720928 | tf_op jit(solution)/shard_map/ppermute | solution.py:29
  305.8 4.7 collective-permute-start.11
  310.5 32.7 %collective-permute-done.8 = bf16[256,1408]{1,0:T(8,128)(2,1)S(1)} collective-permute-done((bf16[256,1408]{1,0:T(8,128)(2,1)S(1)}, bf16[256,1408]{1,0:T(8,128)(2,1)S(1)}, u32[]{:S(2)}, u32[]{:S(2)}) %collective-permute-start.8) | collective-permute-done | bytes 720928 | tf_op jit(solution)/shard_map/ppermute | solution.py:29
  343.2 2.5 collective-permute-start.9
  345.7 2.2 collective-permute-start.12
  347.9 38.5 %collective-permute-done.9 = bf16[256,1408]{1,0:T(8,128)(2,1)S(1)} collective-permute-done((bf16[256,1408]{1,0:T(8,128)(2,1)S(1)}, bf16[256,1408]{1,0:T(8,128)(2,1)S(1)}, u32[]{:S(2)}, u32[]{:S(2)}) %collective-permute-start.9) | collective-permute-done | bytes 720928 | tf_op jit(solution)/shard_map/ppermute | solution.py:29
  386.4 3.3 collective-permute-start.10
  391.1 42.0 %collective-permute-done.10 = bf16[256,1408]{1,0:T(8,128)(2,1)S(1)} collective-permute-done((bf16[256,1408]{1,0:T(8,128)(2,1)S(1)}, bf16[256,1408]{1,0:T(8,128)(2,1)S(1)}, u32[]{:S(2)}, u32[]{:S(2)}) %collective-permute-start.10) | collective-permute-done | bytes 720928 | tf_op jit(solution)/shard_map/ppermute | solution.py:29
  440.6 2.1 fusion.14
  446.4 11.6 %all-gather.9.cloned.1.call-done = bf16[2048,1408]{1,0:T(8,128)(2,1)} async-done(((bf16[256,1408]{1,0:T(8,128)(2,1)}), bf16[2048,1408]{1,0:T(8,128)(2,1)}) %all-gather.9.cloned.1.call-update) | async-done | bytes 5767184 | tf_op jit(solution)/shard_map/all_gather | solution.py:39
  458.0 4.8 fusion.33
  462.8 88.6 %all-gather.11.cloned.1.call-done = bf16[1408,2048]{1,0:T(8,128)(2,1)} async-done(((bf16[1408,256]{1,0:T(8,128)(2,1)}), bf16[1408,2048]{1,0:T(8,128)(2,1)}) %all-gather.11.cloned.1.call-update) | async-done | bytes 5767184 | tf_op jit(solution)/shard_map/all_gather | solution.py:46
  551.4 10.8 %convolution_convert_fusion = bf16[320,2048]{1,0:T(8,128)(2,1)} fusion(bf16[1408,2048]{1,0:T(8,128)(2,1)} %all-gather.11.cloned.1.call-done, f32[320,1408]{1,0:T(8,128)S(1)} %fusion.33, bf16[320,2048]{1,0:T(8,128)(2,1)S(1)} %add_convert_fusion.1, s32[]{:T(128)S(6)} %select_n.13, bf16[2048,1408]{1,0:T(8,128)(2,1)} %constant_dynamic-update-slice_fusion.8), kind=kOutput, calls=%fused_computation.9 | convolution fusion | flops 3705880576 | bytes 15958020 | tf_op jit(solution)/shard_map/dot_general | solution.py:44
  562.2 18.2 %all-reduce.5.cloned.1.call-done = bf16[320,2048]{1,0:T(8,128)(2,1)} async-done(((bf16[320,2048]{1,0:T(8,128)(2,1)}), bf16[320,2048]{1,0:T(8,128)(2,1)}) %all-reduce.5.cloned.1.call-update) | async-done | bytes 1310736 | tf_op jit(solution)/shard_map/psum | solution.py:55
  580.4 2.0 fusion.15
  583.2 1.9 add_convert_fusion
  (72 shorter events, 22.0 us)
Async XLA Ops:
  6.5 172.4 %all-gather.5.cloned.1.call-start = ((), (), s32[]{:S(2)}) async-start(), calls=%async_computation | async-start | bytes 6488064 | tf_op jit(solution)/shard_map/all_gather | solution.py:39
  7.3 266.7 %all-gather.7.cloned.1.call-start = ((), (), s32[]{:S(2)}) async-start(), calls=%async_computation.1 | async-start | bytes 6488064 | tf_op jit(solution)/shard_map/all_gather | solution.py:46
  8.0 432.6 %all-reduce.3.cloned.1.call-start = ((), (), s32[]{:S(2)}) async-start(), calls=%async_computation.2 | async-start | bytes 2621440 | tf_op jit(solution)/shard_map/psum | solution.py:55
  8.1 27.6 %collective-permute-start = (bf16[256,1408]{1,0:T(8,128)(2,1)}, bf16[256,1408]{1,0:T(8,128)(2,1)S(1)}, u32[]{:S(2)}, u32[]{:S(2)}) collective-permute-start(bf16[256,1408]{1,0:T(8,128)(2,1)} %param.18), channel_id=1, source_target_pairs={{0,2},{2,4},{4,6},{6,8},{8,10},{10,12},{12,14},{14,0},{1,3},{3,5},... | collective-permute-start | bytes 2162696 | tf_op jit(solution)/shard_map/ppermute | solution.py:29
  35.6 33.6 %collective-permute-start.1 = (bf16[256,1408]{1,0:T(8,128)(2,1)S(1)}, bf16[256,1408]{1,0:T(8,128)(2,1)S(1)}, u32[]{:S(2)}, u32[]{:S(2)}) collective-permute-start(bf16[256,1408]{1,0:T(8,128)(2,1)S(1)} %collective-permute-done), channel_id=1, source_target_pairs={{0,2},{2,4},{4,6},{6,8},{8,10},{10,12},{12,14},{14,0},{1,3},{3,5},... | collective-permute-start | bytes 2162696 | tf_op jit(solution)/shard_map/ppermute | solution.py:29
  36.1 33.2 %collective-permute-start.4 = (bf16[256,1408]{1,0:T(8,128)(2,1)}, bf16[256,1408]{1,0:T(8,128)(2,1)S(1)}, u32[]{:S(2)}, u32[]{:S(2)}) collective-permute-start(bf16[256,1408]{1,0:T(8,128)(2,1)} %param.18), channel_id=1, source_target_pairs={{0,14},{2,0},{4,2},{6,4},{8,6},{10,8},{12,10},{14,12},{1,15},{3,1}... | collective-permute-start | bytes 2162696 | tf_op jit(solution)/shard_map/ppermute | solution.py:32
  69.2 45.8 %collective-permute-start.2 = (bf16[256,1408]{1,0:T(8,128)(2,1)S(1)}, bf16[256,1408]{1,0:T(8,128)(2,1)}, u32[]{:S(2)}, u32[]{:S(2)}) collective-permute-start(bf16[256,1408]{1,0:T(8,128)(2,1)S(1)} %collective-permute-done.1), channel_id=1, source_target_pairs={{0,2},{2,4},{4,6},{6,8},{8,10},{10,12},{12,14},{14,0},{1,3},{3,5},... | collective-permute-start | bytes 2162696 | tf_op jit(solution)/shard_map/ppermute | solution.py:29
  69.2 48.3 %collective-permute-start.5 = (bf16[256,1408]{1,0:T(8,128)(2,1)S(1)}, bf16[256,1408]{1,0:T(8,128)(2,1)S(1)}, u32[]{:S(2)}, u32[]{:S(2)}) collective-permute-start(bf16[256,1408]{1,0:T(8,128)(2,1)S(1)} %collective-permute-done.4), channel_id=1, source_target_pairs={{0,14},{2,0},{4,2},{6,4},{8,6},{10,8},{12,10},{14,12},{1,15},{3,1}... | collective-permute-start | bytes 2162696 | tf_op jit(solution)/shard_map/ppermute | solution.py:32
  115.0 46.5 %collective-permute-start.3 = (bf16[256,1408]{1,0:T(8,128)(2,1)}, bf16[256,1408]{1,0:T(8,128)(2,1)}, u32[]{:S(2)}, u32[]{:S(2)}) collective-permute-start(bf16[256,1408]{1,0:T(8,128)(2,1)} %collective-permute-done.2), channel_id=1, source_target_pairs={{0,2},{2,4},{4,6},{6,8},{8,10},{10,12},{12,14},{14,0},{1,3},{3,5},... | collective-permute-start | bytes 2162696 | tf_op jit(solution)/shard_map/ppermute | solution.py:29
  117.6 49.9 %copy-start.4 = (bf16[256,1408]{1,0:T(8,128)(2,1)S(1)}, bf16[256,1408]{1,0:T(8,128)(2,1)}, u32[]{:S(2)}) copy-start(bf16[256,1408]{1,0:T(8,128)(2,1)} %param.18) | copy-start | bytes 2162692
  117.6 52.6 %collective-permute-start.6 = (bf16[256,1408]{1,0:T(8,128)(2,1)S(1)}, bf16[256,1408]{1,0:T(8,128)(2,1)S(1)}, u32[]{:S(2)}, u32[]{:S(2)}) collective-permute-start(bf16[256,1408]{1,0:T(8,128)(2,1)S(1)} %collective-permute-done.5), channel_id=1, source_target_pairs={{0,14},{2,0},{4,2},{6,4},{8,6},{10,8},{12,10},{14,12},{1,15},{3,1}... | collective-permute-start | bytes 2162696 | tf_op jit(solution)/shard_map/ppermute | solution.py:32
  167.5 11.4 %copy-start.2 = (bf16[320,2048]{1,0:T(8,128)(2,1)S(1)}, bf16[320,2048]{1,0:T(8,128)(2,1)}, u32[]{:S(2)}) copy-start(bf16[320,2048]{1,0:T(8,128)(2,1)} %param.16) | copy-start | bytes 3932164
  284.7 1.2 copy-start.5
  284.7 173.2 %all-gather.9.cloned.1.call-start = ((), (), s32[]{:S(2)}) async-start(), calls=%async_computation.3 | async-start | bytes 6488064 | tf_op jit(solution)/shard_map/all_gather | solution.py:39
  285.3 266.1 %all-gather.11.cloned.1.call-start = ((), (), s32[]{:S(2)}) async-start(), calls=%async_computation.4 | async-start | bytes 6488064 | tf_op jit(solution)/shard_map/all_gather | solution.py:46
  285.9 294.5 %all-reduce.5.cloned.1.call-start = ((), (), s32[]{:S(2)}) async-start(), calls=%async_computation.5 | async-start | bytes 2621440 | tf_op jit(solution)/shard_map/psum | solution.py:55
  286.0 19.9 %collective-permute-start.7 = (bf16[256,1408]{1,0:T(8,128)(2,1)S(1)}, bf16[256,1408]{1,0:T(8,128)(2,1)S(1)}, u32[]{:S(2)}, u32[]{:S(2)}) collective-permute-start(bf16[256,1408]{1,0:T(8,128)(2,1)S(1)} %copy-done.5), channel_id=1, source_target_pairs={{0,2},{2,4},{4,6},{6,8},{8,10},{10,12},{12,14},{14,0},{1,3},{3,5},... | collective-permute-start | bytes 2162696 | tf_op jit(solution)/shard_map/ppermute | solution.py:29
  305.8 37.4 %collective-permute-start.8 = (bf16[256,1408]{1,0:T(8,128)(2,1)S(1)}, bf16[256,1408]{1,0:T(8,128)(2,1)S(1)}, u32[]{:S(2)}, u32[]{:S(2)}) collective-permute-start(bf16[256,1408]{1,0:T(8,128)(2,1)S(1)} %collective-permute-done.7), channel_id=1, source_target_pairs={{0,2},{2,4},{4,6},{6,8},{8,10},{10,12},{12,14},{14,0},{1,3},{3,5},... | collective-permute-start | bytes 2162696 | tf_op jit(solution)/shard_map/ppermute | solution.py:29
  305.8 39.9 %collective-permute-start.11 = (bf16[256,1408]{1,0:T(8,128)(2,1)S(1)}, bf16[256,1408]{1,0:T(8,128)(2,1)S(1)}, u32[]{:S(2)}, u32[]{:S(2)}) collective-permute-start(bf16[256,1408]{1,0:T(8,128)(2,1)S(1)} %copy-done.5), channel_id=1, source_target_pairs={{0,14},{2,0},{4,2},{6,4},{8,6},{10,8},{12,10},{14,12},{1,15},{3,1}... | collective-permute-start | bytes 2162696 | tf_op jit(solution)/shard_map/ppermute | solution.py:32
  343.2 43.2 %collective-permute-start.9 = (bf16[256,1408]{1,0:T(8,128)(2,1)S(1)}, bf16[256,1408]{1,0:T(8,128)(2,1)S(1)}, u32[]{:S(2)}, u32[]{:S(2)}) collective-permute-start(bf16[256,1408]{1,0:T(8,128)(2,1)S(1)} %collective-permute-done.8), channel_id=1, source_target_pairs={{0,2},{2,4},{4,6},{6,8},{8,10},{10,12},{12,14},{14,0},{1,3},{3,5},... | collective-permute-start | bytes 2162696 | tf_op jit(solution)/shard_map/ppermute | solution.py:29
  345.7 44.1 %collective-permute-start.12 = (bf16[256,1408]{1,0:T(8,128)(2,1)S(1)}, bf16[256,1408]{1,0:T(8,128)(2,1)S(1)}, u32[]{:S(2)}, u32[]{:S(2)}) collective-permute-start(bf16[256,1408]{1,0:T(8,128)(2,1)S(1)} %collective-permute-done.11), channel_id=1, source_target_pairs={{0,14},{2,0},{4,2},{6,4},{8,6},{10,8},{12,10},{14,12},{1,15},{3,1}... | collective-permute-start | bytes 2162696 | tf_op jit(solution)/shard_map/ppermute | solution.py:32
  386.4 46.8 %collective-permute-start.10 = (bf16[256,1408]{1,0:T(8,128)(2,1)S(1)}, bf16[256,1408]{1,0:T(8,128)(2,1)S(1)}, u32[]{:S(2)}, u32[]{:S(2)}) collective-permute-start(bf16[256,1408]{1,0:T(8,128)(2,1)S(1)} %collective-permute-done.9), channel_id=1, source_target_pairs={{0,2},{2,4},{4,6},{6,8},{8,10},{10,12},{12,14},{14,0},{1,3},{3,5},... | collective-permute-start | bytes 2162696 | tf_op jit(solution)/shard_map/ppermute | solution.py:29
  389.7 49.9 %collective-permute-start.13 = (bf16[256,1408]{1,0:T(8,128)(2,1)S(1)}, bf16[256,1408]{1,0:T(8,128)(2,1)S(1)}, u32[]{:S(2)}, u32[]{:S(2)}) collective-permute-start(bf16[256,1408]{1,0:T(8,128)(2,1)S(1)} %collective-permute-done.12), channel_id=1, source_target_pairs={{0,14},{2,0},{4,2},{6,4},{8,6},{10,8},{12,10},{14,12},{1,15},{3,1}... | collective-permute-start | bytes 2162696 | tf_op jit(solution)/shard_map/ppermute | solution.py:32
  440.6 2.9 copy-start.1
  440.6 2.1 copy-start.3
  440.6 2.9 copy-start.6
  440.6 2.9 copy-start.7
  444.8 0.7 copy-start.8
  444.8 0.7 copy-start.9
  562.2 21.0 %copy-start.10 = (f32[2048]{0:T(1024)S(1)}, f32[2048]{0:T(1024)}, u32[]{:S(2)}) copy-start(f32[2048]{0:T(1024)} %param.29) | copy-start | bytes 24580
  562.2 21.0 %copy-start.11 = (f32[2048]{0:T(1024)S(1)}, f32[2048]{0:T(1024)}, u32[]{:S(2)}) copy-start(f32[2048]{0:T(1024)} %param.28) | copy-start | bytes 24580
  580.4 2.0 copy-start
Sparse Core Ops, SparseCore 0:
  9.5 169.3 all-gather.4
  180.9 92.9 all-gather.6
  284.9 18.0 all-reduce.2
  305.0 152.9 all-gather.8
  459.8 91.4 all-gather.10
  562.3 18.0 all-reduce.4
